TPU v7x, 256 devices: a whole 4x4x8 slice. The times are simulated.
256 devices in a mesh: dp: 4 (over y), kv: 32 (over z, x), tp: 2 (over core).
Axes of the slice: x: 4, y: 4, z: 8, core: 2. Of those that a mesh axis runs over, the one named last changes fastest.
Arguments:
- tokens: bfloat16 [16, 16, 2048], P('dp', None, 'kv'), may hold values from -6 to 6
- norm_gain: float32 [2048], P('kv'), may hold values from 0.1 to 1.9
- w_query: bfloat16 [2048, 1024], P('kv', 'tp'), may hold values from -0.125 to 0.125
- w_key: bfloat16 [2048, 1024], P('kv', 'tp'), may hold values from -0.125 to 0.125
- w_value: bfloat16 [2048, 1024], P('kv', 'tp'), may hold values from -0.125 to 0.125
- w_forget: bfloat16 [2048, 16], replicated, may hold values from -0.125 to 0.125
- forget_bias: float32 [16], replicated, may hold values from -2 to 4
- query_gain: float32 [64], replicated, may hold values from 0.1 to 1.9
- key_gain: float32 [64], replicated, may hold values from 0.1 to 1.9
- head_gain: float32 [64], replicated, may hold values from 0.1 to 1.9
- w_out: bfloat16 [1024, 2048], P('tp', 'kv'), may hold values from -0.1875 to 0.1875
- key_cache: bfloat16 [16, 16384, 1024], P('dp', 'kv', 'tp'), may hold values from -240 to 240
- value_cache: bfloat16 [16, 16384, 1024], P('dp', 'kv', 'tp'), may hold values from -6 to 6
- gate_cache: float32 [16, 16, 16384], P('dp', 'tp', 'kv'), may hold values from -1922 to 0, as said below
- lengths: int32 [16], P('dp'), may hold values from 15341 to 16364
- accepted: int32 [16], P('dp'), may hold values from 0 to 4
- parents: int32 [16, 16], P('dp'), may hold values from -1 to 14, as said below
Outputs:
- layer_out: bfloat16 [16, 16, 2048], P('dp', None, 'kv')
- new_keys: bfloat16 [16, 16384, 1024], P('dp', 'kv', 'tp')
- new_values: bfloat16 [16, 16384, 1024], P('dp', 'kv', 'tp')
- proposal_gates: float32 [16, 16, 16], P('dp', None, 'tp')
Inputs may be any that keep to these rules, and one draw needn't show every extreme that they name: `gate_cache`: each entry is the running sum of log forget gates up to its position, so entries never rise along positions; entries at and after lengths hold the last step's proposals in order. `parents`: proposal 0 follows the last accepted token (parent -1); every other proposal's parent is one of the three proposals before it.
All inputs are finite; a program needn't handle non-finite values.
Results may differ from a plain program's by a relative error of at most 0.0051.
The roundings to bfloat16 on the way count: a program that leaves them out, or rounds other values in their place, can miss the bound.
Values may be sent and summed in bfloat16 or wider, within the bound.
No kernel may reach another device: no remote copies, remote signals or barrier semaphores. Data moves between devices by JAX's collectives and lax.ppermute only.
A program may use at most 64 MiB of HBM per device.

v0:
```python
import jax
import jax.numpy as jnp
from jax import lax
from jax.sharding import PartitionSpec as P

EPSILON = 1e-06
MASKED = -1e30


def padded_to(lines, devices):
    spare = -lines.shape[0] % devices
    if not spare:
        return lines
    return jnp.concatenate([lines, jnp.zeros((spare, *lines.shape[1:]), lines.dtype)])


def from_everyone(array, axis):
    devices = lax.axis_size(axis)
    return lax.all_to_all(
        jnp.broadcast_to(array[None], (devices, *array.shape)), axis, 0, 0, tiled=True
    )


def joined_along(parts, dim):
    parts = jnp.moveaxis(parts, 0, dim)
    lengths = parts.shape
    return parts.reshape(*lengths[:dim], lengths[dim] * lengths[dim + 1], *lengths[dim + 2 :])


def collect(array, axis, dim):
    parts = from_everyone(array, axis)
    return joined_along(parts, dim)


def cut_along(array, dim, devices):
    before, after = (array.shape[:dim], array.shape[dim + 1 :])
    return jnp.moveaxis(array.reshape(*before, devices, -1, *after), dim, 0)


def summed_on_arrival(array, axis, dim):
    parts = cut_along(array, dim, lax.axis_size(axis))
    arrived = lax.all_to_all(parts, axis, split_axis=0, concat_axis=0, tiled=True)
    return arrived.sum(axis=0)


def total_of(array, axes):
    padded = padded_to(array, lax.axis_size(axes))
    whole = collect(summed_on_arrival(padded, axes, 0), axes, 0)
    return lax.slice_in_dim(whole, 0, len(array)).reshape(array.shape)


def packed_total(arrays, axis):
    ends = [0]
    for a in arrays:
        ends.append(ends[-1] + a.size)
    total = total_of(jnp.concatenate([a.ravel() for a in arrays]), axis)
    return tuple((total[b:e].reshape(a.shape) for a, b, e in zip(arrays, ends, ends[1:])))


def of_everyone(array, axis):
    return from_everyone(array, axis).astype(jnp.float32).sum(axis=0)


def head_norm(head_rows, gain_vec):
    mean_square = jnp.mean(head_rows * head_rows, axis=-1, keepdims=True)
    return head_rows * lax.rsqrt(mean_square + EPSILON) * gain_vec


def ancestry(parents):
    count_all = parents.shape[1]
    step_ids = jnp.arange(count_all, dtype=jnp.int32)
    step_matrix = (parents[:, :, None] == step_ids[None, None, :]).astype(jnp.float32)
    identity = jnp.broadcast_to(jnp.eye(count_all, dtype=jnp.float32), step_matrix.shape)

    def extend(turn_index, ancestors):
        return identity + jnp.einsum(
            "sij,sjk->sik", step_matrix, ancestors, precision=lax.Precision.HIGHEST
        )

    return lax.fori_loop(0, count_all, extend, identity)


def combine(earlier, later):
    earlier_max, earlier_total, earlier_sum = earlier
    later_max, later_total, later_sum = later
    row_max = jnp.maximum(earlier_max, later_max)
    earlier_scale = jnp.exp(earlier_max - row_max)
    later_scale = jnp.exp(later_max - row_max)
    spread = earlier_max.shape + (-1,)
    joined = (
        earlier_sum.reshape(spread) * earlier_scale[..., None]
        + later_sum.reshape(spread) * later_scale[..., None]
    )
    return (
        row_max,
        earlier_total * earlier_scale + later_total * later_scale,
        joined.reshape(earlier_sum.shape),
    )


def block_part(scores, live_mask, block_values):
    seq_count, heads_local, prop_count, key_count = scores.shape
    row_max = jnp.max(scores, axis=3)
    weights = jnp.where(live_mask, jnp.exp(scores - row_max[..., None]), 0.0)
    row_total = jnp.sum(weights, axis=3)
    weighted = jnp.einsum(
        "shpk,skhd->sphd",
        weights.astype(jnp.bfloat16),
        block_values,
        preferred_element_type=jnp.float32,
    )
    return (
        jnp.transpose(row_max, (0, 2, 1)),
        jnp.transpose(row_total, (0, 2, 1)),
        weighted.reshape(seq_count, prop_count, -1),
    )


def finish_rows(row_sums, inverse, query_gain, key_gain, heads_local):
    head_width = row_sums.shape[1] // 3
    head_size = head_width // heads_local
    row_count = row_sums.shape[0]
    raw_sums = row_sums * inverse[:, None]
    queries = head_norm(
        raw_sums[:, :head_width].reshape(row_count, heads_local, head_size), query_gain
    )
    keyed = head_norm(
        raw_sums[:, head_width : 2 * head_width].reshape(row_count, heads_local, head_size),
        key_gain,
    )
    return jnp.concatenate(
        [
            queries.reshape(row_count, head_width),
            keyed.reshape(row_count, head_width),
            raw_sums[:, 2 * head_width :],
        ],
        axis=1,
    ).astype(jnp.bfloat16)


def flatten_part(part_triple, rows_all):
    part_max, part_total, part_sum = part_triple
    return (
        part_max.reshape(rows_all, -1),
        part_total.reshape(rows_all, -1),
        part_sum.reshape(rows_all, -1),
    )


def shards(
    tokens,
    norm_gain,
    w_query,
    w_key,
    w_value,
    w_forget,
    forget_bias,
    query_gain,
    key_gain,
    head_gain,
    w_out,
    key_cache,
    value_cache,
    gate_cache,
    lengths,
    accepted,
    parents,
):
    seq_count, prop_count, width_in = tokens.shape
    pos_dev = key_cache.shape[1]
    heads_local = gate_cache.shape[1]
    head_width = key_cache.shape[2]
    head_size = head_width // heads_local
    rows_all = seq_count * prop_count
    full_width = w_forget.shape[0]
    kv_index = lax.axis_index("kv")
    tp_index = lax.axis_index("tp")
    flattened = tokens.reshape(rows_all, width_in).astype(jnp.float32)
    squares = jnp.sum(flattened * flattened, axis=1)
    scaled = (flattened * norm_gain).astype(jnp.bfloat16)
    w_rows = lax.dynamic_slice_in_dim(w_forget, kv_index * width_in, width_in, 0)
    gate_part = jnp.dot(scaled, w_rows, preferred_element_type=jnp.float32)
    w_joined = jnp.concatenate([w_query, w_key, w_value], axis=1)
    summed, gate_sum, square_sum = packed_total(
        (jnp.dot(scaled, w_joined, preferred_element_type=jnp.float32), gate_part, squares), "kv"
    )
    inverse = lax.rsqrt(square_sum / full_width + EPSILON)
    joined = finish_rows(summed, inverse, query_gain, key_gain, heads_local)
    log_all = jax.nn.log_sigmoid(gate_sum * inverse[:, None] + forget_bias)
    log_own = lax.dynamic_slice_in_dim(log_all, tp_index * heads_local, heads_local, 1)
    log_own = log_own.reshape(seq_count, prop_count, heads_local)
    queries = joined[:, :head_width].reshape(seq_count, prop_count, heads_local, head_size)
    keys_new = joined[:, head_width : 2 * head_width].reshape(
        seq_count, prop_count, heads_local, head_size
    )
    values_new = joined[:, 2 * head_width :].reshape(seq_count, prop_count, heads_local, head_size)
    ancestors = ancestry(parents)
    path_sum = jnp.einsum("sij,sjh->sih", ancestors, log_own, precision=lax.Precision.HIGHEST)
    base_pos = lengths + accepted
    positions = kv_index * pos_dev + jnp.arange(pos_dev, dtype=jnp.int32)
    score_scale = head_size ** (-0.5)
    cached_keys = key_cache.reshape(seq_count, pos_dev, heads_local, head_size)
    cached_values = value_cache.reshape(seq_count, pos_dev, heads_local, head_size)
    scores = jnp.einsum("sphd,skhd->shpk", queries, cached_keys, preferred_element_type=jnp.float32)
    scores = scores * score_scale - gate_cache[:, :, None, :]
    live_mask = (positions[None, :] < base_pos[:, None])[:, None, None, :]
    scores = jnp.where(live_mask, scores, MASKED)
    local_part = block_part(scores, live_mask, cached_values)
    hit_mask = positions[None, :] == (base_pos - 1)[:, None]
    boundary_local = jnp.sum(jnp.where(hit_mask[:, None, :], gate_cache, 0.0), axis=2)
    tree_live = (ancestors > 0.5)[:, None, :, :]
    owner_mask = jnp.any(hit_mask, axis=1)
    tree_scores = jnp.einsum(
        "sphd,sjhd->shpj", queries, keys_new, preferred_element_type=jnp.float32
    )
    tree_scores = (
        tree_scores * score_scale
        - jnp.transpose(path_sum, (0, 2, 1))[:, :, None, :]
        - boundary_local[:, :, None, None]
    )
    tree_scores = jnp.where(tree_live, tree_scores, MASKED)
    tree_max, tree_total, tree_sum = block_part(tree_scores, tree_live, values_new)
    tree_max = jnp.where(owner_mask[:, None, None], tree_max, MASKED)
    tree_total = jnp.where(owner_mask[:, None, None], tree_total, 0.0)
    tree_sum = jnp.where(owner_mask[:, None, None], tree_sum, 0.0)
    partial_value = combine(local_part, (tree_max, tree_total, tree_sum))
    flat_max, flat_total, flat_sum = flatten_part(partial_value, rows_all)
    got_max, got_total, got_sum = (
        lax.all_to_all(flat_max[None], "kv", split_axis=1, concat_axis=0, tiled=True),
        lax.all_to_all(flat_total[None], "kv", split_axis=1, concat_axis=0, tiled=True),
        lax.all_to_all(flat_sum[None], "kv", split_axis=1, concat_axis=0, tiled=True),
    )
    top = jnp.max(got_max, axis=0)
    factors = jnp.exp(got_max - top[None])
    own_rows = got_max.shape[1]
    summed_rows = jnp.sum(
        got_sum.reshape(got_sum.shape[0], own_rows, heads_local, head_size) * factors[..., None],
        axis=0,
    )
    merged = (top, jnp.sum(got_total * factors, axis=0), summed_rows.reshape(own_rows, head_width))
    row_max, row_total, weighted = merged
    attended = weighted.reshape(own_rows, heads_local, head_size) / row_total[..., None]
    own_normed = head_norm(attended, head_gain).astype(jnp.bfloat16).reshape(own_rows, head_width)
    normed = collect(own_normed, "kv", 0)
    out_term = jnp.dot(normed, w_out, preferred_element_type=jnp.float32)
    layer_out = (
        of_everyone(out_term.astype(jnp.bfloat16), "tp").astype(jnp.float32).astype(jnp.bfloat16)
    )
    layer_out = layer_out.reshape(seq_count, prop_count, -1)
    new_rows = jnp.concatenate(
        [
            keys_new.reshape(seq_count, prop_count, head_width),
            values_new.reshape(seq_count, prop_count, head_width),
        ],
        axis=2,
    )
    slot_index = positions[None, :, None] - base_pos[:, None, None]
    placing = slot_index == jnp.arange(prop_count, dtype=jnp.int32)[None, None, :]
    written = jnp.einsum(
        "skp,spc->skc", placing.astype(jnp.bfloat16), new_rows, preferred_element_type=jnp.float32
    ).astype(jnp.bfloat16)
    hit_rows = jnp.any(placing, axis=2)[..., None]
    new_keys = jnp.where(hit_rows, written[..., :head_width], key_cache)
    new_values = jnp.where(hit_rows, written[..., head_width:], value_cache)
    return (layer_out, new_keys, new_values, log_own)


def solution(mesh):
    placed = (
        P("dp", None, "kv"),
        P("kv"),
        P("kv", "tp"),
        P("kv", "tp"),
        P("kv", "tp"),
        P(),
        P(),
        P(),
        P(),
        P(),
        P("tp", "kv"),
        P("dp", "kv", "tp"),
        P("dp", "kv", "tp"),
        P("dp", "tp", "kv"),
        P("dp"),
        P("dp"),
        P("dp", None),
    )
    return jax.shard_map(
        shards,
        mesh=mesh,
        in_specs=placed,
        out_specs=(
            P("dp", None, "kv"),
            P("dp", "kv", "tp"),
            P("dp", "kv", "tp"),
            P("dp", None, "tp"),
        ),
        check_vma=False,
    )
```

profile of v0, /device:TPU:1, one launch (start us, length us, event | category | flops | bytes accessed | tf_op | source)
XLA Modules:
  0.0 130.6 jit_solution(2430243420172668842)
XLA Ops:
  0.7 0.8 multiply_reduce_fusion.2
  1.6 0.7 fusion.48
  2.3 0.9 fusion.53
  3.3 1.1 fusion.23
  4.5 1.3 %all_to_all.43 = f32[32,1,3106]{2,1,0:T(1,128)} reshape(f32[99392]{0:T(1024)S(1)} %pad_maximum_fusion) | data formatting | bytes 795136 | tf_op jit(solution)/shard_map/all_to_all | solution.py:42
  5.8 11.9 %all-to-all-start = ((f32[32,1,3106]{2,1,0:T(1,128)}), f32[32,1,3106]{2,1,0:T(1,128)S(1)}, u32[]{:S(2)}, u32[]{:S(2)}) async-start(f32[32,1,3106]{2,1,0:T(1,128)} %all_to_all.43), calls=%async_computation | async-start | bytes 819200 | tf_op jit(solution)/shard_map/all_to_all | solution.py:42
  17.7 4.2 %while.11 = (s32[]{:T(128)}, f32[4,16,16]{2,1,0:T(8,128)S(1)}, s32[4,16]{1,0:T(4,128)S(1)}, f32[16,16]{1,0:T(8,128)S(1)}, s32[]{:T(128)}) while((s32[]{:T(128)}, f32[4,16,16]{2,1,0:T(8,128)S(1)}, s32[4,16]{1,0:T(4,128)S(1)}, f32[16,16]{1,0:T(8,128)S(1)}, s32[]{:T(128)}) %tuple.48), condition=%wide.region_6.7_spmd.clone, body=%wide.region_5.6_spmd.clone.sunk | while | flops 199682 | bytes 17725 | solution.py:80
  22.1 0.6 mul.237
  22.9 2.4 %copy.142 = bf16[4,512,512]{1,2,0:T(8,128)(2,1)} copy(bf16[4,512,512]{2,1,0:T(8,128)(2,1)S(1)} %copy-done.2) | data formatting | bytes 4194304 | tf_op args[11]
  25.3 2.8 %copy.144 = bf16[4,512,512]{1,2,0:T(8,128)(2,1)S(1)} copy(bf16[4,512,512]{2,1,0:T(8,128)(2,1)} %param.31) | data formatting | bytes 4194304 | tf_op args[12]
  28.1 3.5 %all-to-all-done = f32[32,1,3106]{2,1,0:T(1,128)S(1)} async-done(((f32[32,1,3106]{2,1,0:T(1,128)}), f32[32,1,3106]{2,1,0:T(1,128)S(1)}, u32[]{:S(2)}, u32[]{:S(2)}) %all-to-all-start) | async-done | bytes 397600 | tf_op jit(solution)/shard_map/all_to_all | solution.py:42
  31.6 0.2 reduce_sum.108
  31.9 1.0 broadcast_in_dim.148
  32.8 5.7 %all-to-all-start.1 = ((f32[32,1,3106]{2,1,0:T(1,128)}), f32[32,1,3106]{2,1,0:T(1,128)S(1)}, u32[]{:S(2)}, u32[]{:S(2)}) async-start(f32[32,1,3106]{2,1,0:T(1,128)} %broadcast_in_dim.148), calls=%async_computation.1 | async-start | bytes 819200 | tf_op jit(solution)/shard_map/all_to_all | solution.py:19
  38.7 0.6 fusion.35
  39.3 1.3 fusion.64
  40.6 0.7 select_reduce_fusion
  41.3 10.9 %all-to-all-done.1 = f32[32,1,3106]{2,1,0:T(1,128)S(1)} async-done(((f32[32,1,3106]{2,1,0:T(1,128)}), f32[32,1,3106]{2,1,0:T(1,128)S(1)}, u32[]{:S(2)}, u32[]{:S(2)}) %all-to-all-start.1) | async-done | bytes 397600 | tf_op jit(solution)/shard_map/all_to_all | solution.py:19
  52.1 1.0 reduce.4
  53.4 3.5 %slice.41 = f32[6212,16]{1,0:T(8,128)} reshape(f32[32,3106]{1,0:T(8,128)S(1)} %reduce.4) | data formatting | bytes 795136 | tf_op jit(solution)/shard_map/slice | solution.py:57
  58.7 0.8 reshape.283
  59.4 0.8 fusion.65
  60.6 2.1 %fusion.67 = (f32[4,8,16]{2,1,0:T(8,128)S(1)}, f32[4,8,16,512]{3,2,1,0:T(8,128)S(1)}) fusion(f32[4,8,512]{2,1,0:T(8,128)S(1)} %copy-done.7, bf16[4,512,8,64]{1,3,2,0:T(8,128)(2,1)} %bitcast.63, bf16[4,16,8,64]{3,2,1,0:T(8,128)(2,1)S(1)} %reshape.280, pred[4,512]{1,0:T(4,128)(4,1)S(1)} %copy-done.14), kind=kOutput, calls=%fused_computation.107 | convolution fusion | flops 34602496 | bytes 3280896 | tf_op jit(solution)/shard_map/sphd,skhd->shpk/dot_general | solution.py:204
  62.8 0.3 fusion.15
  63.1 0.2 fusion.68
  63.4 0.7 copy-done.4
  64.2 0.7 fusion.49
  64.9 0.7 copy.166
  65.6 5.6 %all-to-all-start.4 = ((f32[1,64,8]{2,0,1:T(1,128)}), f32[1,64,8]{2,0,1:T(1,128)}, u32[]{:S(2)}, u32[]{:S(2)}) async-start(f32[1,64,8]{2,0,1:T(1,128)} %bitcast.13), calls=%async_computation.4 | async-start | bytes 65536 | tf_op jit(solution)/shard_map/all_to_all | solution.py:230
  71.2 1.4 %fusion.13 = f32[4,16,8,64]{3,1,2,0:T(8,128)S(1)} fusion(bf16[4,512,8,64]{1,3,2,0:T(8,128)(2,1)S(1)} %bitcast.62, f32[4,8,16,512]{3,2,1,0:T(8,128)S(1)} %get-tuple-element.96, f32[4,8,16]{2,1,0:T(8,128)S(1)} %get-tuple-element.95, pred[4,512]{1,0:T(4,128)(4,1)} %get-tuple-element.94, f32[4,16,8]{1,2,0:T(8,128)} %get-tuple-element.80), kind=kOutput, calls=%fused_computation.20 | convolution fusion | flops 34373632 | bytes 3282944 | tf_op jit(solution)/shard_map/shpk,skhd->sphd/dot_general | solution.py:106
  72.6 0.9 slice.73
  73.7 1.4 %copy.165 = f32[4,16,8]{2,1,0:T(8,128)} copy(f32[4,16,8]{1,2,0:T(8,128)} %get-tuple-element.81) | data formatting | bytes 4096 | tf_op jit(solution)/shard_map/broadcast_in_dim;reshape | solution.py:229
  75.1 4.7 %all-to-all-done.4 = f32[1,64,8]{2,0,1:T(1,128)} async-done(((f32[1,64,8]{2,0,1:T(1,128)}), f32[1,64,8]{2,0,1:T(1,128)}, u32[]{:S(2)}, u32[]{:S(2)}) %all-to-all-start.4) | async-done | bytes 2080 | tf_op jit(solution)/shard_map/all_to_all | solution.py:230
  79.8 4.4 %all-to-all-start.3 = ((f32[1,64,8]{2,0,1:T(1,128)}), f32[1,64,8]{2,0,1:T(1,128)S(1)}, u32[]{:S(2)}, u32[]{:S(2)}) async-start(f32[1,64,8]{2,0,1:T(1,128)} %bitcast.9), calls=%async_computation.3 | async-start | bytes 65536 | tf_op jit(solution)/shard_map/all_to_all | solution.py:229
  84.2 1.2 fusion.10
  85.6 0.8 broadcast_in_dim_reshape_reshape.4
  86.4 6.5 %all-to-all-done.3 = f32[1,64,8]{2,0,1:T(1,128)S(1)} async-done(((f32[1,64,8]{2,0,1:T(1,128)}), f32[1,64,8]{2,0,1:T(1,128)S(1)}, u32[]{:S(2)}, u32[]{:S(2)}) %all-to-all-start.3) | async-done | bytes 2080 | tf_op jit(solution)/shard_map/all_to_all | solution.py:229
  92.9 4.0 %all-to-all-start.2 = ((f32[1,64,512]{2,0,1:T(1,128)}), f32[1,64,512]{2,0,1:T(1,128)S(1)}, u32[]{:S(2)}, u32[]{:S(2)}) async-start(f32[1,64,512]{2,0,1:T(1,128)} %broadcast_in_dim_reshape_reshape.4), calls=%async_computation.2 | async-start | bytes 262144 | tf_op jit(solution)/shard_map/all_to_all | solution.py:231
  97.0 3.2 %convolution_convert_fusion = bf16[4,512,1024]{2,1,0:T(8,128)(2,1)} fusion(bf16[4,16,512]{2,1,0:T(8,128)(2,1)S(1)} %bitcast.65, bf16[4,16,512]{2,1,0:T(8,128)(2,1)S(1)} %bitcast.64, s32[4,512]{1,0:T(4,128)S(1)} %copy-done.12), kind=kOutput, calls=%fused_computation.6 | convolution fusion | flops 69500928 | bytes 4333568 | tf_op jit(solution)/shard_map/skp,spc->skc/dot_general | solution.py:259
  100.3 0.8 multiply_reduce_fusion.1
  101.6 4.6 %all-to-all-done.2 = f32[1,64,512]{2,0,1:T(1,128)S(1)} async-done(((f32[1,64,512]{2,0,1:T(1,128)}), f32[1,64,512]{2,0,1:T(1,128)S(1)}, u32[]{:S(2)}, u32[]{:S(2)}) %all-to-all-start.2) | async-done | bytes 131104 | tf_op jit(solution)/shard_map/all_to_all | solution.py:231
  106.8 0.7 broadcast_in_dim.162
  107.5 4.4 %all-to-all-start.5 = ((bf16[32,2,512]{2,1,0:T(2,128)(2,1)}), bf16[32,2,512]{2,1,0:T(2,128)(2,1)S(1)}, u32[]{:S(2)}, u32[]{:S(2)}) async-start(bf16[32,2,512]{2,1,0:T(2,128)(2,1)} %broadcast_in_dim.162), calls=%async_computation.5 | async-start | bytes 131072 | tf_op jit(solution)/shard_map/all_to_all | solution.py:19
  111.9 4.4 %slice_select_fusion = (bf16[4,512,512]{2,1,0:T(8,128)(2,1)}, bf16[4,512,512]{2,1,0:T(8,128)(2,1)}) fusion(bf16[4,512,512]{2,1,0:T(8,128)(2,1)S(1)} %copy-done.1, bf16[4,512,1024]{2,1,0:T(8,128)(2,1)} %convolution_convert_fusion, pred[4,512]{1,0:T(4,128)(4,1)S(1)} %copy-done.16, bf16[4,512,512]{2,1,0:T(8,128)(2,1)} %param.30), kind=kLoop, calls=%fused_computation.7 | loop fusion | flops 2097152 | bytes 12584960 | tf_op jit(solution)/shard_map/jit(_where)/select_n | solution.py:264
  116.4 0.7 copy.151
  117.1 3.7 %all-to-all-done.5 = bf16[32,2,512]{2,1,0:T(2,128)(2,1)S(1)} async-done(((bf16[32,2,512]{2,1,0:T(2,128)(2,1)}), bf16[32,2,512]{2,1,0:T(2,128)(2,1)S(1)}, u32[]{:S(2)}, u32[]{:S(2)}) %all-to-all-start.5) | async-done | bytes 65568 | tf_op jit(solution)/shard_map/all_to_all | solution.py:19
  121.0 8.8 %all_to_all.61 = bf16[2,2,2048]{2,1,0:T(2,128)(2,1)S(1)} all-to-all(bf16[2,2,2048]{2,1,0:T(2,128)(2,1)S(1)} %reshape.291), channel_id=1, replica_groups=mesh['dp'=4,'kv'=32,'tp'=2] {'tp'}, dimensions={0} | all-to-all | bytes 32768 | tf_op jit(solution)/shard_map/all_to_all | solution.py:19
  130.0 0.6 reduce_sum.118
  (141 shorter events, 8.4 us)
Async XLA Ops:
  0.6 120.1 %copy-start = (bf16[512,64]{0,1:T(8,128)(2,1)S(1)}, bf16[512,64]{0,1:T(8,128)(2,1)}, u32[]{:S(2)}) copy-start(bf16[512,64]{0,1:T(8,128)(2,1)} %param.29) | copy-start | bytes 196612
  0.6 17.1 %copy-start.13 = (s32[4,16]{1,0:T(4,128)S(1)}, s32[4,16]{1,0:T(4,128)}, u32[]{:S(2)}) copy-start(s32[4,16]{1,0:T(4,128)} %param.35) | copy-start | bytes 772
  4.4 17.6 %copy-start.20 = (f32[64]{0:T(128)S(1)}, f32[64]{0:T(128)}, u32[]{:S(2)}) copy-start(f32[64]{0:T(128)} %param.26) | copy-start | bytes 772
  4.4 17.7 %copy-start.21 = (f32[64]{0:T(128)S(1)}, f32[64]{0:T(128)}, u32[]{:S(2)}) copy-start(f32[64]{0:T(128)} %param.27) | copy-start | bytes 772
  4.4 17.7 %copy-start.22 = (f32[64]{0:T(128)S(1)}, f32[64]{0:T(128)}, u32[]{:S(2)}) copy-start(f32[64]{0:T(128)} %param.28) | copy-start | bytes 772
  4.4 18.5 %copy-start.2 = (bf16[4,512,512]{2,1,0:T(8,128)(2,1)S(1)}, bf16[4,512,512]{2,1,0:T(8,128)(2,1)}, u32[]{:S(2)}) copy-start(bf16[4,512,512]{2,1,0:T(8,128)(2,1)} %param.30) | copy-start | bytes 6291460
  5.8 25.8 %all-to-all-start = ((f32[32,1,3106]{2,1,0:T(1,128)}), f32[32,1,3106]{2,1,0:T(1,128)S(1)}, u32[]{:S(2)}, u32[]{:S(2)}) async-start(f32[32,1,3106]{2,1,0:T(1,128)} %all_to_all.43), calls=%async_computation | async-start | bytes 819200 | tf_op jit(solution)/shard_map/all_to_all | solution.py:42
  22.9 40.5 %copy-start.10 = (pred[4,16,16]{1,2,0:T(8,128)(4,1)}, pred[4,16,16]{1,2,0:T(8,128)(4,1)S(1)}, u32[]{:S(2)}) copy-start(pred[4,16,16]{1,2,0:T(8,128)(4,1)S(1)} %copy.145) | copy-start | bytes 3076
  25.3 2.8 %copy-start.23 = (s32[4]{0:T(128)S(1)}, s32[4]{0:T(128)}, u32[]{:S(2)}) copy-start(s32[4]{0:T(128)} %param.33) | copy-start | bytes 52
  25.3 2.8 %copy-start.24 = (s32[4]{0:T(128)S(1)}, s32[4]{0:T(128)}, u32[]{:S(2)}) copy-start(s32[4]{0:T(128)} %param.34) | copy-start | bytes 52
  25.3 15.3 %copy-start.7 = (f32[4,8,512]{2,1,0:T(8,128)S(1)}, f32[4,8,512]{2,1,0:T(8,128)}, u32[]{:S(2)}) copy-start(f32[4,8,512]{2,1,0:T(8,128)} %param.32) | copy-start | bytes 196612
  32.8 19.3 %all-to-all-start.1 = ((f32[32,1,3106]{2,1,0:T(1,128)}), f32[32,1,3106]{2,1,0:T(1,128)S(1)}, u32[]{:S(2)}, u32[]{:S(2)}) async-start(f32[32,1,3106]{2,1,0:T(1,128)} %broadcast_in_dim.148), calls=%async_computation.1 | async-start | bytes 819200 | tf_op jit(solution)/shard_map/all_to_all | solution.py:19
  38.7 14.7 %copy-start.11 = (s32[4,512]{1,0:T(4,128)}, s32[4,512]{1,0:T(4,128)S(1)}, u32[]{:S(2)}) copy-start(s32[4,512]{1,0:T(4,128)S(1)} %broadcast_subtract_fusion) | copy-start | bytes 24580
  57.1 1.6 %copy-start.3 = (f32[64,1536]{1,0:T(8,128)}, f32[64,1536]{1,0:T(8,128)S(1)}, u32[]{:S(2)}) copy-start(f32[64,1536]{1,0:T(8,128)S(1)} %broadcast_multiply_fusion) | copy-start | bytes 1179652
  57.1 2.3 %copy-start.19 = (f32[16]{0:T(128)S(1)}, f32[16]{0:T(128)}, u32[]{:S(2)}) copy-start(f32[16]{0:T(128)} %param.25) | copy-start | bytes 196
  57.1 3.5 %copy-start.14 = (pred[4,512]{1,0:T(4,128)(4,1)S(1)}, pred[4,512]{1,0:T(4,128)(4,1)}, u32[]{:S(2)}) copy-start(pred[4,512]{1,0:T(4,128)(4,1)} %get-tuple-element.94) | copy-start | bytes 6148
  60.4 2.7 %copy-start.5 = (f32[64,8]{1,0:T(8,128)}, f32[64,8]{1,0:T(8,128)S(1)}, u32[]{:S(2)}) copy-start(f32[64,8]{1,0:T(8,128)S(1)} %fusion.42) | copy-start | bytes 6148
  60.6 2.5 %copy-start.9 = (bf16[4,16,8,64]{3,2,1,0:T(8,128)(2,1)S(1)}, bf16[4,16,8,64]{3,2,1,0:T(8,128)(2,1)}, u32[]{:S(2)}) copy-start(bf16[4,16,8,64]{3,2,1,0:T(8,128)(2,1)} %reshape.283) | copy-start | bytes 196612
  60.6 2.5 %copy-start.18 = (f32[4,8]{1,0:T(4,128)S(1)}, f32[4,8]{1,0:T(4,128)}, u32[]{:S(2)}) copy-start(f32[4,8]{1,0:T(4,128)} %select_reduce_fusion) | copy-start | bytes 388
  60.6 3.5 %copy-start.17 = (pred[4]{0:T(512)(128)(4,1)S(1)}, pred[4]{0:T(512)(128)(4,1)}, u32[]{:S(2)}) copy-start(pred[4]{0:T(512)(128)(4,1)} %get-tuple-element.82) | copy-start | bytes 16
  63.4 0.7 copy-start.4
  63.4 7.8 %copy-start.8 = (f32[4,8,16]{2,1,0:T(8,128)}, f32[4,8,16]{2,1,0:T(8,128)S(1)}, u32[]{:S(2)}) copy-start(f32[4,8,16]{2,1,0:T(8,128)S(1)} %get-tuple-element.97) | copy-start | bytes 6148
  65.6 14.3 %all-to-all-start.4 = ((f32[1,64,8]{2,0,1:T(1,128)}), f32[1,64,8]{2,0,1:T(1,128)}, u32[]{:S(2)}, u32[]{:S(2)}) async-start(f32[1,64,8]{2,0,1:T(1,128)} %bitcast.13), calls=%async_computation.4 | async-start | bytes 65536 | tf_op jit(solution)/shard_map/all_to_all | solution.py:230
  72.6 24.4 %copy-start.12 = (s32[4,512]{1,0:T(4,128)S(1)}, s32[4,512]{1,0:T(4,128)}, u32[]{:S(2)}) copy-start(s32[4,512]{1,0:T(4,128)} %copy-done.11) | copy-start | bytes 24580
  79.8 13.1 %all-to-all-start.3 = ((f32[1,64,8]{2,0,1:T(1,128)}), f32[1,64,8]{2,0,1:T(1,128)S(1)}, u32[]{:S(2)}, u32[]{:S(2)}) async-start(f32[1,64,8]{2,0,1:T(1,128)} %bitcast.9), calls=%async_computation.3 | async-start | bytes 65536 | tf_op jit(solution)/shard_map/all_to_all | solution.py:229
  92.9 13.3 %all-to-all-start.2 = ((f32[1,64,512]{2,0,1:T(1,128)}), f32[1,64,512]{2,0,1:T(1,128)S(1)}, u32[]{:S(2)}, u32[]{:S(2)}) async-start(f32[1,64,512]{2,0,1:T(1,128)} %broadcast_in_dim_reshape_reshape.4), calls=%async_computation.2 | async-start | bytes 262144 | tf_op jit(solution)/shard_map/all_to_all | solution.py:231
  97.0 9.8 %copy-start.15 = (f32[512]{0:T(512)S(1)}, f32[512]{0:T(512)}, u32[]{:S(2)}) copy-start(f32[512]{0:T(512)} %mul.237) | copy-start | bytes 6148
  97.0 14.9 %copy-start.1 = (bf16[4,512,512]{2,1,0:T(8,128)(2,1)S(1)}, bf16[4,512,512]{2,1,0:T(8,128)(2,1)}, u32[]{:S(2)}) copy-start(bf16[4,512,512]{2,1,0:T(8,128)(2,1)} %param.31) | copy-start | bytes 6291460
  97.0 14.9 %copy-start.16 = (pred[4,512]{1,0:T(4,128)(4,1)S(1)}, pred[4,512]{1,0:T(4,128)(4,1)}, u32[]{:S(2)}) copy-start(pred[4,512]{1,0:T(4,128)(4,1)} %fusion.35) | copy-start | bytes 6148
  107.5 13.2 %all-to-all-start.5 = ((bf16[32,2,512]{2,1,0:T(2,128)(2,1)}), bf16[32,2,512]{2,1,0:T(2,128)(2,1)S(1)}, u32[]{:S(2)}, u32[]{:S(2)}) async-start(bf16[32,2,512]{2,1,0:T(2,128)(2,1)} %broadcast_in_dim.162), calls=%async_computation.5 | async-start | bytes 131072 | tf_op jit(solution)/shard_map/all_to_all | solution.py:19
  111.9 4.5 %copy-start.6 = (f32[64,8]{1,0:T(8,128)S(1)}, f32[64,8]{1,0:T(8,128)}, u32[]{:S(2)}) copy-start(f32[64,8]{1,0:T(8,128)} %copy-done.5) | copy-start | bytes 6148
where the time goes:
time: 132 us; the launch traced here: 131 us
  starting transfers between devices  36 us (27%)
  waiting for transfers between devices  34 us (26%)
  local copies, waits for them, and re-layouts  21.5 us (16%)
  other arithmetic  14.3 us (11%)
  matrix products  14.2 us (11%)
  blocking collectives  8.85 us (7%)
    all_to_all x2, waiting for transfers between devices, from_everyone(): lax.all_to_all(jnp.broadcast_to(array[None], (devices, *array.shape)), ax...  14.6 us
    all_to_all x1, starting transfers between devices, summed_on_arrival(): lax.all_to_all(parts, axis, split_axis=0, concat_axis=0, tiled=True)  11.9 us
    all_to_all x2, starting transfers between devices, from_everyone(): lax.all_to_all(jnp.broadcast_to(array[None], (devices, *array.shape)), ax...  10.1 us
    all_to_all x1, blocking collectives, from_everyone(): lax.all_to_all(jnp.broadcast_to(array[None], (devices, *array.shape)), ax...  8.85 us
    all_to_all x1, waiting for transfers between devices, shards(): lax.all_to_all(flat_max[None], 'kv', split_axis=1, concat_axis=0, tiled=T...  6.53 us
    unnamed x54, local copies, waits for them, and re-layouts  6.18 us
    all_to_all x1, starting transfers between devices, shards(): lax.all_to_all(flat_total[None], 'kv', split_axis=1, concat_axis=0, tiled...  5.57 us
    all_to_all x1, waiting for transfers between devices, shards(): lax.all_to_all(flat_total[None], 'kv', split_axis=1, concat_axis=0, tiled...  4.74 us
  transfers between devices with their start and end apart: 6, of which 6 were waited for; matrix products, arithmetic and copies ran while one was open for 22% of the time, Pallas kernels for 0%

commit v1 on v0

--- a/solution.py
+++ b/solution.py
@@ -226,7 +226,12 @@
     partial_value = combine(local_part, (tree_max, tree_total, tree_sum))
     flat_max, flat_total, flat_sum = flatten_part(partial_value, rows_all)
     got_max, got_total, got_sum = (
-        lax.all_to_all(flat_max[None], "kv", split_axis=1, concat_axis=0, tiled=True),
+        jnp.concatenate(
+            lax.all_to_all(
+                jnp.stack(jnp.split(flat_max[None], lax.axis_size("kv"), axis=1)), "kv", 0, 0
+            ),
+            axis=0,
+        ),
         lax.all_to_all(flat_total[None], "kv", split_axis=1, concat_axis=0, tiled=True),
         lax.all_to_all(flat_sum[None], "kv", split_axis=1, concat_axis=0, tiled=True),
     )

time: 132 us -> 152 us (1.15)
  local copies, waits for them, and re-layouts: 21.5 us -> 41.2 us
  starting transfers between devices: 36 us -> 40.8 us
  waiting for transfers between devices: 34 us -> 29.3 us
    split x0 -> x34, local copies, waits for them, and re-layouts: none -> 20.1 us  [shards(): jnp.split(flat_max[None], lax.axis_size('kv'), axis=1)]
    all_to_all x1, starting transfers between devices: 4.4 us -> 9.15 us  [shards(): lax.all_to_all(jnp.stack(jnp.split(flat_max[None], lax.axis_size('kv'), a...]
    all_to_all x1, waiting for transfers between devices: 4.74 us -> 0.01 us  [shards(): lax.all_to_all(flat_total[None], 'kv', split_axis=1, concat_axis=0, tiled...]
    unnamed x54 -> x151, local copies, waits for them, and re-layouts: 6.18 us -> 7.07 us
  transfers between devices with their start and end apart: 6 -> 6, of which waited for: 6 -> 5; matrix products, arithmetic and copies ran while one was open for 22% -> 32% of each run, Pallas kernels for 0% -> 0%
where the time goes in v1:
time: 152 us; the launch traced here: 151 us
  local copies, waits for them, and re-layouts  41.2 us (27%)
  starting transfers between devices  40.8 us (27%)
  waiting for transfers between devices  29.3 us (19%)
  other arithmetic  14.4 us (9%)
  matrix products  14.3 us (9%)
  blocking collectives  8.81 us (6%)
  between operations  1.89 us (1%)
    split x34, local copies, waits for them, and re-layouts, shards(): jnp.split(flat_max[None], lax.axis_size('kv'), axis=1)  20.1 us
    all_to_all x2, waiting for transfers between devices, from_everyone(): lax.all_to_all(jnp.broadcast_to(array[None], (devices, *array.shape)), ax...  14.5 us
    all_to_all x1, starting transfers between devices, summed_on_arrival(): lax.all_to_all(parts, axis, split_axis=0, concat_axis=0, tiled=True)  11.9 us
    all_to_all x2, starting transfers between devices, from_everyone(): lax.all_to_all(jnp.broadcast_to(array[None], (devices, *array.shape)), ax...  10.2 us
    all_to_all x1, starting transfers between devices, shards(): lax.all_to_all(jnp.stack(jnp.split(flat_max[None], lax.axis_size('kv'), a...  9.15 us
    all_to_all x1, blocking collectives, from_everyone(): lax.all_to_all(jnp.broadcast_to(array[None], (devices, *array.shape)), ax...  8.81 us
    unnamed x151, local copies, waits for them, and re-layouts  7.07 us
    all_to_all x1, waiting for transfers between devices, shards(): lax.all_to_all(jnp.stack(jnp.split(flat_max[None], lax.axis_size('kv'), a...  6.52 us
  transfers between devices with their start and end apart: 6, of which 5 were waited for; matrix products, arithmetic and copies ran while one was open for 32% of the time, Pallas kernels for 0%

profile of v1, /device:TPU:1, one launch (start us, length us, event | category | flops | bytes accessed | tf_op | source)
XLA Modules:
  0.0 151.1 jit_solution(8580714541217813342)
XLA Ops:
  0.7 0.8 multiply_reduce_fusion.2
  1.6 0.7 fusion.49
  2.3 0.9 fusion.54
  3.3 1.1 fusion.23
  4.5 1.3 all_to_all.37
  5.8 11.9 %all-to-all-start = ((f32[32,1,3106]{2,1,0:T(1,128)}), f32[32,1,3106]{2,1,0:T(1,128)S(1)}, u32[]{:S(2)}, u32[]{:S(2)}) async-start(f32[32,1,3106]{2,1,0:T(1,128)} %all_to_all.37), calls=%async_computation | async-start | bytes 819200 | tf_op jit(solution)/shard_map/all_to_all | solution.py:42
  17.7 4.2 %while.11 = (s32[]{:T(128)}, f32[4,16,16]{2,1,0:T(8,128)S(1)}, s32[4,16]{1,0:T(4,128)S(1)}, f32[16,16]{1,0:T(8,128)S(1)}, s32[]{:T(128)}) while((s32[]{:T(128)}, f32[4,16,16]{2,1,0:T(8,128)S(1)}, s32[4,16]{1,0:T(4,128)S(1)}, f32[16,16]{1,0:T(8,128)S(1)}, s32[]{:T(128)}) %tuple.79), condition=%wide.region_6.7_spmd.clone, body=%wide.region_5.6_spmd.clone.sunk | while | flops 199682 | bytes 17725 | solution.py:80
  22.9 2.4 %copy.446 = bf16[4,512,512]{1,2,0:T(8,128)(2,1)} copy(bf16[4,512,512]{2,1,0:T(8,128)(2,1)S(1)} %copy-done.2) | data formatting | bytes 4194304 | tf_op args[11]
  25.3 2.8 %copy.448 = bf16[4,512,512]{1,2,0:T(8,128)(2,1)S(1)} copy(bf16[4,512,512]{2,1,0:T(8,128)(2,1)} %param.31) | data formatting | bytes 4194304 | tf_op args[12]
  28.1 3.5 %all-to-all-done = f32[32,1,3106]{2,1,0:T(1,128)S(1)} async-done(((f32[32,1,3106]{2,1,0:T(1,128)}), f32[32,1,3106]{2,1,0:T(1,128)S(1)}, u32[]{:S(2)}, u32[]{:S(2)}) %all-to-all-start) | async-done | bytes 397600 | tf_op jit(solution)/shard_map/all_to_all | solution.py:42
  31.9 1.0 broadcast_in_dim.148
  32.8 5.7 %all-to-all-start.1 = ((f32[32,1,3106]{2,1,0:T(1,128)}), f32[32,1,3106]{2,1,0:T(1,128)S(1)}, u32[]{:S(2)}, u32[]{:S(2)}) async-start(f32[32,1,3106]{2,1,0:T(1,128)} %broadcast_in_dim.148), calls=%async_computation.1 | async-start | bytes 819200 | tf_op jit(solution)/shard_map/all_to_all | solution.py:19
  39.3 1.4 fusion.66
  40.7 0.7 select_reduce_fusion
  41.3 10.8 %all-to-all-done.1 = f32[32,1,3106]{2,1,0:T(1,128)S(1)} async-done(((f32[32,1,3106]{2,1,0:T(1,128)}), f32[32,1,3106]{2,1,0:T(1,128)S(1)}, u32[]{:S(2)}, u32[]{:S(2)}) %all-to-all-start.1) | async-done | bytes 397600 | tf_op jit(solution)/shard_map/all_to_all | solution.py:19
  52.2 1.0 reduce.5
  53.4 3.5 %slice.41 = f32[6212,16]{1,0:T(8,128)} reshape(f32[32,3106]{1,0:T(8,128)S(1)} %reduce.5) | data formatting | bytes 795136 | tf_op jit(solution)/shard_map/slice | solution.py:57
  58.6 0.8 reshape.286
  59.4 0.8 fusion.67
  60.6 2.1 %fusion.71 = (f32[4,8,16]{2,1,0:T(8,128)S(1)}, f32[4,8,16,512]{3,2,1,0:T(8,128)S(1)}) fusion(f32[4,8,512]{2,1,0:T(8,128)S(1)} %copy-done.7, bf16[4,512,8,64]{1,3,2,0:T(8,128)(2,1)} %bitcast.132, bf16[4,16,8,64]{3,2,1,0:T(8,128)(2,1)S(1)} %reshape.283, pred[4,512]{1,0:T(4,128)(4,1)S(1)} %copy-done.16), kind=kOutput, calls=%fused_computation.142 | convolution fusion | flops 34602496 | bytes 3280896 | tf_op jit(solution)/shard_map/sphd,skhd->shpk/dot_general | solution.py:204
  63.5 0.7 fusion.50
  64.5 0.7 copy.500
  65.2 5.6 %all-to-all-start.4 = ((f32[1,64,8]{2,0,1:T(1,128)}), f32[1,64,8]{2,0,1:T(1,128)}, u32[]{:S(2)}, u32[]{:S(2)}) async-start(f32[1,64,8]{2,0,1:T(1,128)} %bitcast.44), calls=%async_computation.4 | async-start | bytes 65536 | tf_op jit(solution)/shard_map/all_to_all | solution.py:235
  73.3 0.7 copy.469
  74.0 0.7 copy.468
  75.9 0.7 copy.465
  79.1 0.7 copy.492
  81.6 0.7 copy.488
  84.2 0.7 copy.484
  86.1 0.7 copy.481
  89.9 0.7 copy.475
  90.6 0.7 copy.474
  91.6 1.4 fusion.13
  94.3 0.9 slice.73
  95.4 9.2 %all-to-all-start.3 = ((f32[32,1,2,8]{3,2,1,0:T(2,128)}), f32[32,1,2,8]{3,2,1,0:T(2,128)S(1)}, u32[]{:S(2)}, u32[]{:S(2)}) async-start(f32[32,1,2,8]{3,2,1,0:T(2,128)} %copy-done.15), calls=%async_computation.3 | async-start | bytes 65536 | tf_op jit(solution)/shard_map/all_to_all | solution.py:230
  104.5 1.2 fusion.10
  105.9 0.8 broadcast_in_dim_reshape_reshape.4
  106.7 6.5 %all-to-all-done.3 = f32[32,1,2,8]{3,2,1,0:T(2,128)S(1)} async-done(((f32[32,1,2,8]{3,2,1,0:T(2,128)}), f32[32,1,2,8]{3,2,1,0:T(2,128)S(1)}, u32[]{:S(2)}, u32[]{:S(2)}) %all-to-all-start.3) | async-done | bytes 2080 | tf_op jit(solution)/shard_map/all_to_all | solution.py:230
  113.2 4.0 %all-to-all-start.2 = ((f32[1,64,512]{2,0,1:T(1,128)}), f32[1,64,512]{2,0,1:T(1,128)S(1)}, u32[]{:S(2)}, u32[]{:S(2)}) async-start(f32[1,64,512]{2,0,1:T(1,128)} %broadcast_in_dim_reshape_reshape.4), calls=%async_computation.2 | async-start | bytes 262144 | tf_op jit(solution)/shard_map/all_to_all | solution.py:236
  117.3 3.3 %convolution_convert_fusion = bf16[4,512,1024]{2,1,0:T(8,128)(2,1)} fusion(bf16[4,16,512]{2,1,0:T(8,128)(2,1)S(1)} %bitcast.134, bf16[4,16,512]{2,1,0:T(8,128)(2,1)S(1)} %bitcast.133, s32[4,512]{1,0:T(4,128)S(1)} %copy-done.12), kind=kOutput, calls=%fused_computation.6 | convolution fusion | flops 69500928 | bytes 4333568 | tf_op jit(solution)/shard_map/skp,spc->skc/dot_general | solution.py:264
  120.6 0.8 multiply_reduce_fusion.1
  121.9 4.8 %all-to-all-done.2 = f32[1,64,512]{2,0,1:T(1,128)S(1)} async-done(((f32[1,64,512]{2,0,1:T(1,128)}), f32[1,64,512]{2,0,1:T(1,128)S(1)}, u32[]{:S(2)}, u32[]{:S(2)}) %all-to-all-start.2) | async-done | bytes 131104 | tf_op jit(solution)/shard_map/all_to_all | solution.py:236
  127.3 0.7 broadcast_in_dim.162
  128.0 4.4 %all-to-all-start.5 = ((bf16[32,2,512]{2,1,0:T(2,128)(2,1)}), bf16[32,2,512]{2,1,0:T(2,128)(2,1)S(1)}, u32[]{:S(2)}, u32[]{:S(2)}) async-start(bf16[32,2,512]{2,1,0:T(2,128)(2,1)} %broadcast_in_dim.162), calls=%async_computation.5 | async-start | bytes 131072 | tf_op jit(solution)/shard_map/all_to_all | solution.py:19
  132.4 4.4 %slice_select_fusion = (bf16[4,512,512]{2,1,0:T(8,128)(2,1)}, bf16[4,512,512]{2,1,0:T(8,128)(2,1)}) fusion(bf16[4,512,512]{2,1,0:T(8,128)(2,1)S(1)} %copy-done.1, bf16[4,512,1024]{2,1,0:T(8,128)(2,1)} %convolution_convert_fusion, pred[4,512]{1,0:T(4,128)(4,1)S(1)} %copy-done.18, bf16[4,512,512]{2,1,0:T(8,128)(2,1)} %param.30), kind=kLoop, calls=%fused_computation.7 | loop fusion | flops 2097152 | bytes 12584960 | tf_op jit(solution)/shard_map/jit(_where)/select_n | solution.py:269
  136.9 0.7 copy.455
  137.6 3.7 %all-to-all-done.5 = bf16[32,2,512]{2,1,0:T(2,128)(2,1)S(1)} async-done(((bf16[32,2,512]{2,1,0:T(2,128)(2,1)}), bf16[32,2,512]{2,1,0:T(2,128)(2,1)S(1)}, u32[]{:S(2)}, u32[]{:S(2)}) %all-to-all-start.5) | async-done | bytes 65568 | tf_op jit(solution)/shard_map/all_to_all | solution.py:19
  141.5 8.8 %all_to_all.54 = bf16[2,2,2048]{2,1,0:T(2,128)(2,1)S(1)} all-to-all(bf16[2,2,2048]{2,1,0:T(2,128)(2,1)S(1)} %reshape.295), channel_id=1, replica_groups=mesh['dp'=4,'kv'=32,'tp'=2] {'tp'}, dimensions={0} | all-to-all | bytes 32768 | tf_op jit(solution)/shard_map/all_to_all | solution.py:19
  (274 shorter events, 27.0 us)
Async XLA Ops:
  0.6 140.6 %copy-start = (bf16[512,64]{0,1:T(8,128)(2,1)S(1)}, bf16[512,64]{0,1:T(8,128)(2,1)}, u32[]{:S(2)}) copy-start(bf16[512,64]{0,1:T(8,128)(2,1)} %param.29) | copy-start | bytes 196612
  0.6 17.1 %copy-start.13 = (s32[4,16]{1,0:T(4,128)S(1)}, s32[4,16]{1,0:T(4,128)}, u32[]{:S(2)}) copy-start(s32[4,16]{1,0:T(4,128)} %param.35) | copy-start | bytes 772
  4.4 17.6 %copy-start.53 = (f32[64]{0:T(128)S(1)}, f32[64]{0:T(128)}, u32[]{:S(2)}) copy-start(f32[64]{0:T(128)} %param.26) | copy-start | bytes 772
  4.4 17.7 %copy-start.54 = (f32[64]{0:T(128)S(1)}, f32[64]{0:T(128)}, u32[]{:S(2)}) copy-start(f32[64]{0:T(128)} %param.27) | copy-start | bytes 772
  4.4 17.7 %copy-start.55 = (f32[64]{0:T(128)S(1)}, f32[64]{0:T(128)}, u32[]{:S(2)}) copy-start(f32[64]{0:T(128)} %param.28) | copy-start | bytes 772
  4.4 18.5 %copy-start.2 = (bf16[4,512,512]{2,1,0:T(8,128)(2,1)S(1)}, bf16[4,512,512]{2,1,0:T(8,128)(2,1)}, u32[]{:S(2)}) copy-start(bf16[4,512,512]{2,1,0:T(8,128)(2,1)} %param.30) | copy-start | bytes 6291460
  5.8 25.8 %all-to-all-start = ((f32[32,1,3106]{2,1,0:T(1,128)}), f32[32,1,3106]{2,1,0:T(1,128)S(1)}, u32[]{:S(2)}, u32[]{:S(2)}) async-start(f32[32,1,3106]{2,1,0:T(1,128)} %all_to_all.37), calls=%async_computation | async-start | bytes 819200 | tf_op jit(solution)/shard_map/all_to_all | solution.py:42
  22.9 40.5 %copy-start.10 = (pred[4,16,16]{1,2,0:T(8,128)(4,1)}, pred[4,16,16]{1,2,0:T(8,128)(4,1)S(1)}, u32[]{:S(2)}) copy-start(pred[4,16,16]{1,2,0:T(8,128)(4,1)S(1)} %copy.449) | copy-start | bytes 3076
  25.3 2.8 %copy-start.56 = (s32[4]{0:T(128)S(1)}, s32[4]{0:T(128)}, u32[]{:S(2)}) copy-start(s32[4]{0:T(128)} %param.33) | copy-start | bytes 52
  25.3 2.8 %copy-start.57 = (s32[4]{0:T(128)S(1)}, s32[4]{0:T(128)}, u32[]{:S(2)}) copy-start(s32[4]{0:T(128)} %param.34) | copy-start | bytes 52
  25.3 15.4 %copy-start.7 = (f32[4,8,512]{2,1,0:T(8,128)S(1)}, f32[4,8,512]{2,1,0:T(8,128)}, u32[]{:S(2)}) copy-start(f32[4,8,512]{2,1,0:T(8,128)} %param.32) | copy-start | bytes 196612
  32.8 19.3 %all-to-all-start.1 = ((f32[32,1,3106]{2,1,0:T(1,128)}), f32[32,1,3106]{2,1,0:T(1,128)S(1)}, u32[]{:S(2)}, u32[]{:S(2)}) async-start(f32[32,1,3106]{2,1,0:T(1,128)} %broadcast_in_dim.148), calls=%async_computation.1 | async-start | bytes 819200 | tf_op jit(solution)/shard_map/all_to_all | solution.py:19
  38.7 14.7 %copy-start.11 = (s32[4,512]{1,0:T(4,128)}, s32[4,512]{1,0:T(4,128)S(1)}, u32[]{:S(2)}) copy-start(s32[4,512]{1,0:T(4,128)S(1)} %broadcast_subtract_fusion) | copy-start | bytes 24580
  57.1 2.4 %copy-start.52 = (f32[16]{0:T(128)S(1)}, f32[16]{0:T(128)}, u32[]{:S(2)}) copy-start(f32[16]{0:T(128)} %param.25) | copy-start | bytes 196
  57.1 3.5 %copy-start.16 = (pred[4,512]{1,0:T(4,128)(4,1)S(1)}, pred[4,512]{1,0:T(4,128)(4,1)}, u32[]{:S(2)}) copy-start(pred[4,512]{1,0:T(4,128)(4,1)} %get-tuple-element.130) | copy-start | bytes 6148
  60.4 2.7 %copy-start.5 = (f32[64,8]{1,0:T(8,128)}, f32[64,8]{1,0:T(8,128)S(1)}, u32[]{:S(2)}) copy-start(f32[64,8]{1,0:T(8,128)S(1)} %fusion.42) | copy-start | bytes 6148
  60.6 2.5 %copy-start.9 = (bf16[4,16,8,64]{3,2,1,0:T(8,128)(2,1)S(1)}, bf16[4,16,8,64]{3,2,1,0:T(8,128)(2,1)}, u32[]{:S(2)}) copy-start(bf16[4,16,8,64]{3,2,1,0:T(8,128)(2,1)} %reshape.286) | copy-start | bytes 196612
  60.6 2.5 %copy-start.51 = (f32[4,8]{1,0:T(4,128)S(1)}, f32[4,8]{1,0:T(4,128)}, u32[]{:S(2)}) copy-start(f32[4,8]{1,0:T(4,128)} %select_reduce_fusion) | copy-start | bytes 388
  60.6 2.9 %copy-start.19 = (pred[4]{0:T(512)(128)(4,1)S(1)}, pred[4]{0:T(512)(128)(4,1)}, u32[]{:S(2)}) copy-start(pred[4]{0:T(512)(128)(4,1)} %get-tuple-element.86) | copy-start | bytes 16
  63.4 28.2 %copy-start.8 = (f32[4,8,16]{2,1,0:T(8,128)}, f32[4,8,16]{2,1,0:T(8,128)S(1)}, u32[]{:S(2)}) copy-start(f32[4,8,16]{2,1,0:T(8,128)S(1)} %get-tuple-element.133) | copy-start | bytes 6148
  65.2 30.2 %all-to-all-start.4 = ((f32[1,64,8]{2,0,1:T(1,128)}), f32[1,64,8]{2,0,1:T(1,128)}, u32[]{:S(2)}, u32[]{:S(2)}) async-start(f32[1,64,8]{2,0,1:T(1,128)} %bitcast.44), calls=%async_computation.4 | async-start | bytes 65536 | tf_op jit(solution)/shard_map/all_to_all | solution.py:235
  91.4 1.9 %copy-start.50 = (f32[1,2,8]{2,1,0:T(2,128)S(1)}, f32[1,2,8]{2,1,0:T(2,128)}, u32[]{:S(2)}) copy-start(f32[1,2,8]{2,1,0:T(2,128)} %copy.474) | copy-start | bytes 196
  91.4 1.9 %copy-start.49 = (f32[1,2,8]{2,1,0:T(2,128)S(1)}, f32[1,2,8]{2,1,0:T(2,128)}, u32[]{:S(2)}) copy-start(f32[1,2,8]{2,1,0:T(2,128)} %copy.475) | copy-start | bytes 196
  91.4 1.9 %copy-start.47 = (f32[1,2,8]{2,1,0:T(2,128)S(1)}, f32[1,2,8]{2,1,0:T(2,128)}, u32[]{:S(2)}) copy-start(f32[1,2,8]{2,1,0:T(2,128)} %copy.476) | copy-start | bytes 196
  91.4 2.0 %copy-start.45 = (f32[1,2,8]{2,1,0:T(2,128)S(1)}, f32[1,2,8]{2,1,0:T(2,128)}, u32[]{:S(2)}) copy-start(f32[1,2,8]{2,1,0:T(2,128)} %copy.477) | copy-start | bytes 196
  91.4 2.0 %copy-start.43 = (f32[1,2,8]{2,1,0:T(2,128)S(1)}, f32[1,2,8]{2,1,0:T(2,128)}, u32[]{:S(2)}) copy-start(f32[1,2,8]{2,1,0:T(2,128)} %copy.478) | copy-start | bytes 196
  91.4 2.0 %copy-start.41 = (f32[1,2,8]{2,1,0:T(2,128)S(1)}, f32[1,2,8]{2,1,0:T(2,128)}, u32[]{:S(2)}) copy-start(f32[1,2,8]{2,1,0:T(2,128)} %copy.479) | copy-start | bytes 196
  91.4 2.0 %copy-start.39 = (f32[1,2,8]{2,1,0:T(2,128)S(1)}, f32[1,2,8]{2,1,0:T(2,128)}, u32[]{:S(2)}) copy-start(f32[1,2,8]{2,1,0:T(2,128)} %copy.480) | copy-start | bytes 196
  91.4 2.0 %copy-start.37 = (f32[1,2,8]{2,1,0:T(2,128)S(1)}, f32[1,2,8]{2,1,0:T(2,128)}, u32[]{:S(2)}) copy-start(f32[1,2,8]{2,1,0:T(2,128)} %copy.481) | copy-start | bytes 196
  91.5 2.0 %copy-start.35 = (f32[1,2,8]{2,1,0:T(2,128)S(1)}, f32[1,2,8]{2,1,0:T(2,128)}, u32[]{:S(2)}) copy-start(f32[1,2,8]{2,1,0:T(2,128)} %copy.482) | copy-start | bytes 196
  91.5 2.0 %copy-start.33 = (f32[1,2,8]{2,1,0:T(2,128)S(1)}, f32[1,2,8]{2,1,0:T(2,128)}, u32[]{:S(2)}) copy-start(f32[1,2,8]{2,1,0:T(2,128)} %copy.483) | copy-start | bytes 196
  91.5 2.0 %copy-start.31 = (f32[1,2,8]{2,1,0:T(2,128)S(1)}, f32[1,2,8]{2,1,0:T(2,128)}, u32[]{:S(2)}) copy-start(f32[1,2,8]{2,1,0:T(2,128)} %copy.484) | copy-start | bytes 196
  91.5 2.1 %copy-start.29 = (f32[1,2,8]{2,1,0:T(2,128)S(1)}, f32[1,2,8]{2,1,0:T(2,128)}, u32[]{:S(2)}) copy-start(f32[1,2,8]{2,1,0:T(2,128)} %copy.485) | copy-start | bytes 196
  91.5 2.1 %copy-start.27 = (f32[1,2,8]{2,1,0:T(2,128)S(1)}, f32[1,2,8]{2,1,0:T(2,128)}, u32[]{:S(2)}) copy-start(f32[1,2,8]{2,1,0:T(2,128)} %copy.486) | copy-start | bytes 196
  91.5 2.1 %copy-start.25 = (f32[1,2,8]{2,1,0:T(2,128)S(1)}, f32[1,2,8]{2,1,0:T(2,128)}, u32[]{:S(2)}) copy-start(f32[1,2,8]{2,1,0:T(2,128)} %copy.487) | copy-start | bytes 196
  91.5 2.1 %copy-start.24 = (f32[1,2,8]{2,1,0:T(2,128)S(1)}, f32[1,2,8]{2,1,0:T(2,128)}, u32[]{:S(2)}) copy-start(f32[1,2,8]{2,1,0:T(2,128)} %copy.488) | copy-start | bytes 196
  91.5 2.1 %copy-start.23 = (f32[1,2,8]{2,1,0:T(2,128)S(1)}, f32[1,2,8]{2,1,0:T(2,128)}, u32[]{:S(2)}) copy-start(f32[1,2,8]{2,1,0:T(2,128)} %copy.489) | copy-start | bytes 196
  91.5 2.1 %copy-start.22 = (f32[1,2,8]{2,1,0:T(2,128)S(1)}, f32[1,2,8]{2,1,0:T(2,128)}, u32[]{:S(2)}) copy-start(f32[1,2,8]{2,1,0:T(2,128)} %copy.490) | copy-start | bytes 196
  91.5 2.1 %copy-start.21 = (f32[1,2,8]{2,1,0:T(2,128)S(1)}, f32[1,2,8]{2,1,0:T(2,128)}, u32[]{:S(2)}) copy-start(f32[1,2,8]{2,1,0:T(2,128)} %copy.491) | copy-start | bytes 196
  91.6 2.1 %copy-start.20 = (f32[1,2,8]{2,1,0:T(2,128)S(1)}, f32[1,2,8]{2,1,0:T(2,128)}, u32[]{:S(2)}) copy-start(f32[1,2,8]{2,1,0:T(2,128)} %copy.492) | copy-start | bytes 196
  93.0 24.3 %copy-start.12 = (s32[4,512]{1,0:T(4,128)S(1)}, s32[4,512]{1,0:T(4,128)}, u32[]{:S(2)}) copy-start(s32[4,512]{1,0:T(4,128)} %copy-done.11) | copy-start | bytes 24580
  95.4 17.9 %all-to-all-start.3 = ((f32[32,1,2,8]{3,2,1,0:T(2,128)}), f32[32,1,2,8]{3,2,1,0:T(2,128)S(1)}, u32[]{:S(2)}, u32[]{:S(2)}) async-start(f32[32,1,2,8]{3,2,1,0:T(2,128)} %copy-done.15), calls=%async_computation.3 | async-start | bytes 65536 | tf_op jit(solution)/shard_map/all_to_all | solution.py:230
  113.2 13.5 %all-to-all-start.2 = ((f32[1,64,512]{2,0,1:T(1,128)}), f32[1,64,512]{2,0,1:T(1,128)S(1)}, u32[]{:S(2)}, u32[]{:S(2)}) async-start(f32[1,64,512]{2,0,1:T(1,128)} %broadcast_in_dim_reshape_reshape.4), calls=%async_computation.2 | async-start | bytes 262144 | tf_op jit(solution)/shard_map/all_to_all | solution.py:236
  117.3 10.0 %copy-start.17 = (f32[512]{0:T(512)S(1)}, f32[512]{0:T(512)}, u32[]{:S(2)}) copy-start(f32[512]{0:T(512)} %mul.237) | copy-start | bytes 6148
  117.3 15.1 %copy-start.1 = (bf16[4,512,512]{2,1,0:T(8,128)(2,1)S(1)}, bf16[4,512,512]{2,1,0:T(8,128)(2,1)}, u32[]{:S(2)}) copy-start(bf16[4,512,512]{2,1,0:T(8,128)(2,1)} %param.31) | copy-start | bytes 6291460
  117.3 15.1 %copy-start.18 = (pred[4,512]{1,0:T(4,128)(4,1)S(1)}, pred[4,512]{1,0:T(4,128)(4,1)}, u32[]{:S(2)}) copy-start(pred[4,512]{1,0:T(4,128)(4,1)} %fusion.35) | copy-start | bytes 6148
  128.0 13.3 %all-to-all-start.5 = ((bf16[32,2,512]{2,1,0:T(2,128)(2,1)}), bf16[32,2,512]{2,1,0:T(2,128)(2,1)S(1)}, u32[]{:S(2)}, u32[]{:S(2)}) async-start(bf16[32,2,512]{2,1,0:T(2,128)(2,1)} %broadcast_in_dim.162), calls=%async_computation.5 | async-start | bytes 131072 | tf_op jit(solution)/shard_map/all_to_all | solution.py:19
  132.4 4.5 %copy-start.6 = (f32[64,8]{1,0:T(8,128)S(1)}, f32[64,8]{1,0:T(8,128)}, u32[]{:S(2)}) copy-start(f32[64,8]{1,0:T(8,128)} %copy-done.5) | copy-start | bytes 6148
  (16 other events, 26.9 us)
